TPU v7x, 32 devices: a whole 2x2x4 slice. The times are simulated.
32 devices in a mesh: grp: 2 (over y), fs: 4 (over z), tp: 4 (over x, core).
Axes of the slice: x: 2, y: 2, z: 4, core: 2. Of those that a mesh axis runs over, the one named last changes fastest.
Arguments:
- tokens: bfloat16 [2048, 2048], P(('grp', 'fs')), parts along dimension 0, may hold values from -6 to 6
- ffn_pre_gain: bfloat16 [2048], replicated, may hold values from 0.099609375 to 1.8984375
- gate_weight: bfloat16 [2048, 5632], P('fs', 'tp'), may hold values from -0.125 to 0.125
- up_weight: bfloat16 [2048, 5632], P('fs', 'tp'), may hold values from -0.125 to 0.125
- down_weight: bfloat16 [5632, 2048], P('tp', 'fs'), may hold values from -0.078125 to 0.078125
- ffn_post_gain: bfloat16 [2048], replicated, may hold values from 0.099609375 to 1.8984375
- mix_pre_gain: bfloat16 [2048], replicated, may hold values from 0.099609375 to 1.8984375
- mix_u_weight: bfloat16 [2048, 2048], P('fs', 'tp'), may hold values from -0.125 to 0.125
- mix_v_weight: bfloat16 [2048, 2048], P('fs', 'tp'), may hold values from -0.125 to 0.125
- spatial_gain: bfloat16 [2048], P('tp'), may hold values from 0.099609375 to 1.8984375
- spatial_weight: bfloat16 [16, 128, 128], P('tp'), may hold values from -0.5 to 0.5
- spatial_bias: bfloat16 [16, 128], P('tp'), may hold values from 0.099609375 to 1.8984375
- mix_out_weight: bfloat16 [2048, 2048], P('tp', 'fs'), may hold values from -0.125 to 0.125
- mix_post_gain: bfloat16 [2048], replicated, may hold values from 0.099609375 to 1.8984375
- late_pre_gain: bfloat16 [2048], replicated, may hold values from 0.099609375 to 1.8984375
- late_post_gain: bfloat16 [2048], replicated, may hold values from 0.099609375 to 1.8984375
Outputs:
- result: bfloat16 [2048, 2048], P(('grp', 'fs')), parts along dimension 0
There are 2 independent parts, one for each index of `grp`. A program takes and returns all parts, laid end to end along the dimension named above; an argument that names none is the same for every part. Nothing has to cross between parts.
All inputs are finite; a program needn't handle non-finite values.
Results may differ from a plain program's by a relative error of at most 0.019.
Values may be sent and summed in bfloat16 or wider, within the bound.
No kernel may reach another device: no remote copies, remote signals or barrier semaphores. Data moves between devices by JAX's collectives and lax.ppermute only.
A program may use at most 128 MiB of HBM per device.

v0:
```python
import jax
import jax.numpy as jnp
from jax import lax
from jax.sharding import PartitionSpec as P

GROUP_WIDTH = 128
BLOCK = 128


def row_norm(values, gain):
    scale = lax.rsqrt(jnp.mean(values * values, axis=-1, keepdims=True) + 1e-06)
    return values * scale * gain.astype(jnp.float32)


def reduce_partial(terms):
    return lax.psum(terms.astype(jnp.bfloat16), "tp").astype(jnp.float32)


def add_branch(stream, terms, gain, factor):
    total = reduce_partial(terms)
    return (stream.astype(jnp.float32) + factor * row_norm(total, gain)).astype(jnp.bfloat16)


def gated_hidden(normed, gate_full, up_full):
    gate = jnp.dot(normed, gate_full, preferred_element_type=jnp.float32)
    upper = jnp.dot(normed, up_full, preferred_element_type=jnp.float32)
    return (jax.nn.silu(gate) * upper).astype(jnp.bfloat16)


def spatial_mix(u_linear, v_linear, spatial_gain, spatial_weight, spatial_bias):
    count = u_linear.shape[0]
    gated_u = jax.nn.gelu(u_linear, approximate=False)
    gating_v = jax.nn.gelu(v_linear, approximate=False)
    groups = gating_v.shape[1] // GROUP_WIDTH
    grouped = gating_v.reshape(count, groups, GROUP_WIDTH)
    centred = grouped - jnp.mean(grouped, axis=-1, keepdims=True)
    vnorm = centred * lax.rsqrt(jnp.mean(centred * centred, axis=-1, keepdims=True) + 1e-05)
    vnorm = (vnorm * spatial_gain.astype(jnp.float32).reshape(groups, GROUP_WIDTH)).astype(
        jnp.bfloat16
    )
    blocks = vnorm.reshape(count // BLOCK, BLOCK, groups, GROUP_WIDTH)
    lower = jnp.tril(jnp.ones((BLOCK, BLOCK), dtype=bool))
    masked = jnp.where(lower[None], spatial_weight, jnp.zeros_like(spatial_weight))
    spatial = jnp.einsum("gts,nsgc->ntgc", masked, blocks, preferred_element_type=jnp.float32)
    spatial = spatial + spatial_bias.astype(jnp.float32).T[None, :, :, None]
    return (gated_u * spatial.reshape(count, groups * GROUP_WIDTH)).astype(jnp.bfloat16)


def shards(
    tokens,
    ffn_pre_gain,
    gate_weight,
    up_weight,
    down_weight,
    ffn_post_gain,
    mix_pre_gain,
    mix_u_weight,
    mix_v_weight,
    spatial_gain,
    spatial_weight,
    spatial_bias,
    mix_out_weight,
    mix_post_gain,
    late_pre_gain,
    late_post_gain,
):
    normed = row_norm(tokens.astype(jnp.float32), ffn_pre_gain).astype(jnp.bfloat16)
    gate_full, up_full = (
        lax.all_gather(gate_weight, "fs", axis=0, tiled=True),
        lax.all_gather(up_weight, "fs", axis=0, tiled=True),
    )
    down_full = lax.all_gather(down_weight, "fs", axis=1, tiled=True)
    hidden = gated_hidden(normed, gate_full, up_full)
    terms = jnp.dot(hidden, down_full, preferred_element_type=jnp.float32)
    first = add_branch(tokens, terms, ffn_post_gain, 0.5)
    normed = row_norm(first.astype(jnp.float32), mix_pre_gain).astype(jnp.bfloat16)
    u_full, v_full = (
        lax.all_gather(mix_u_weight, "fs", axis=0, tiled=True),
        lax.all_gather(mix_v_weight, "fs", axis=0, tiled=True),
    )
    u_linear = jnp.dot(normed, u_full, preferred_element_type=jnp.float32)
    v_linear = jnp.dot(normed, v_full, preferred_element_type=jnp.float32)
    mixed = spatial_mix(u_linear, v_linear, spatial_gain, spatial_weight, spatial_bias)
    out_full = lax.all_gather(mix_out_weight, "fs", axis=1, tiled=True)
    terms = jnp.dot(mixed, out_full, preferred_element_type=jnp.float32)
    second = add_branch(first, terms, mix_post_gain, 1.0)
    normed = row_norm(second.astype(jnp.float32), late_pre_gain).astype(jnp.bfloat16)
    hidden = gated_hidden(normed, gate_full, up_full)
    terms = jnp.dot(hidden, down_full, preferred_element_type=jnp.float32)
    return add_branch(second, terms, late_post_gain, 0.5)


def solution(mesh):
    in_specs = (
        P(("grp", "fs"), None),
        P(),
        P("fs", "tp"),
        P("fs", "tp"),
        P("tp", "fs"),
        P(),
        P(),
        P("fs", "tp"),
        P("fs", "tp"),
        P("tp"),
        P("tp", None, None),
        P("tp", None),
        P("tp", "fs"),
        P(),
        P(),
        P(),
    )
    out_specs = P(("grp", "fs"), None)
    return jax.shard_map(shards, mesh=mesh, in_specs=in_specs, out_specs=out_specs, check_vma=False)
```

profile of v0, /device:TPU:0, one launch (start us, length us, event | category | flops | bytes accessed | tf_op | source)
XLA Modules:
  0.0 620.2 jit_solution(5151979985591970159)
XLA Ops:
  6.5 0.0 copy-start.2
  6.5 0.0 copy-start
  6.5 0.0 all-gather.7.cloned.1.call-start
  6.5 0.7 all-gather.7.cloned.1.call-update
  7.3 0.0 all-gather.11.cloned.1.call-start
  7.3 0.7 all-gather.11.cloned.1.call-update
  8.0 0.0 all-gather.9.cloned.1.call-start
  8.1 0.7 all-gather.9.cloned.1.call-update
  8.7 0.0 all-reduce.4.cloned.1.call-start
  8.8 0.0 copy-done.2
  8.8 0.0 copy-done
  8.8 0.3 fusion.10
  9.1 109.2 %all-gather.7.cloned.1.call-done = bf16[2048,1408]{1,0:T(8,128)(2,1)} async-done(((bf16[512,1408]{1,0:T(8,128)(2,1)}), bf16[2048,1408]{1,0:T(8,128)(2,1)}) %all-gather.7.cloned.1.call-update) | async-done | bytes 5767184 | tf_op jit(solution)/shard_map/all_gather | solution.py:69
  118.3 4.5 fusion.59
  122.8 102.0 %all-gather.11.cloned.1.call-done = bf16[1408,2048]{1,0:T(8,128)(2,1)} async-done(((bf16[1408,512]{1,0:T(8,128)(2,1)}), bf16[1408,2048]{1,0:T(8,128)(2,1)}) %all-gather.11.cloned.1.call-update) | async-done | bytes 5767184 | tf_op jit(solution)/shard_map/all_gather | solution.py:72
  224.9 106.6 %all-gather.9.cloned.1.call-done = bf16[2048,1408]{1,0:T(8,128)(2,1)} async-done(((bf16[512,1408]{1,0:T(8,128)(2,1)}), bf16[2048,1408]{1,0:T(8,128)(2,1)}) %all-gather.9.cloned.1.call-update) | async-done | bytes 5767184 | tf_op jit(solution)/shard_map/all_gather | solution.py:70
  331.4 8.9 %convolution_convert_fusion.2 = bf16[256,2048]{1,0:T(8,128)(2,1)} fusion(bf16[1408,2048]{1,0:T(8,128)(2,1)} %all-gather.11.cloned.1.call-done, bf16[2048,1408]{1,0:T(8,128)(2,1)} %all-gather.9.cloned.1.call-done, f32[256,1408]{1,0:T(8,128)S(1)} %fusion.59, bf16[256,2048]{1,0:T(8,128)(2,1)S(1)} %copy-done, f32[2048]{0:T(1024)S(1)} %convert_element_type.82, ...), kind=kOutput, calls=%fused_computation.21 | convolution fusion | flops 2957574144 | bytes 15082496 | tf_op jit(solution)/shard_map/dot_general | solution.py:74
  340.4 0.0 copy-start.3
  340.4 0.0 all-reduce.4.cloned.1.call-update
  340.4 0.0 all-gather.15.cloned.1.call-start
  340.5 0.5 all-gather.15.cloned.1.call-update
  341.0 0.0 all-gather.13.cloned.1.call-start
  341.0 0.5 all-gather.13.cloned.1.call-update
  341.6 0.0 all-gather.17.cloned.1.call-start
  341.6 0.7 all-gather.17.cloned.1.call-update
  342.3 0.2 all-reduce.6.cloned.1.call-start
  342.6 0.0 copy-done.3
  342.6 0.0 copy-done.4
  342.6 0.0 copy-done.8
  342.6 0.0 copy-done.9
  342.7 32.4 %all-reduce.4.cloned.1.call-done = bf16[256,2048]{1,0:T(8,128)(2,1)} async-done(((bf16[256,2048]{1,0:T(8,128)(2,1)}), bf16[256,2048]{1,0:T(8,128)(2,1)}) %all-reduce.4.cloned.1.call-update) | async-done | bytes 1048592 | tf_op jit(solution)/shard_map/psum | solution.py:16
  375.1 1.5 fusion.2
  376.6 2.0 fusion.14
  378.6 44.1 %all-gather.15.cloned.1.call-done = bf16[2048,512]{1,0:T(8,128)(2,1)} async-done(((bf16[512,512]{1,0:T(8,128)(2,1)}), bf16[2048,512]{1,0:T(8,128)(2,1)}) %all-gather.15.cloned.1.call-update) | async-done | bytes 2097168 | tf_op jit(solution)/shard_map/all_gather | solution.py:79
  422.7 3.4 fusion.28
  426.1 0.2 reshape.99
  426.3 0.0 copy-start.1
  426.3 0.2 reshape.98
  426.5 0.3 reduce_sum.75
  426.8 0.6 multiply_reduce_fusion
  427.5 0.1 copy.36
  427.6 0.1 copy.37
  427.7 0.2 copy.25
  427.9 0.0 copy-done.1
  427.9 0.3 fusion.22
  428.2 0.2 copy.28
  428.5 40.1 %all-gather.13.cloned.1.call-done = bf16[2048,512]{1,0:T(8,128)(2,1)} async-done(((bf16[512,512]{1,0:T(8,128)(2,1)}), bf16[2048,512]{1,0:T(8,128)(2,1)}) %all-gather.13.cloned.1.call-update) | async-done | bytes 2097168 | tf_op jit(solution)/shard_map/all_gather | solution.py:78
  468.6 46.1 %all-gather.17.cloned.1.call-done = bf16[512,2048]{1,0:T(8,128)(2,1)} async-done(((bf16[512,512]{1,0:T(8,128)(2,1)}), bf16[512,2048]{1,0:T(8,128)(2,1)}) %all-gather.17.cloned.1.call-update) | async-done | bytes 2097168 | tf_op jit(solution)/shard_map/all_gather | solution.py:84
  514.7 5.7 convolution_convert_fusion
  520.4 0.0 all-reduce.6.cloned.1.call-update
  520.4 0.3 all-reduce.8.cloned.1.call-start
  520.7 0.0 copy-done.5
  520.7 0.0 copy-done.6
  520.7 34.9 %all-reduce.6.cloned.1.call-done = bf16[256,2048]{1,0:T(8,128)(2,1)} async-done(((bf16[256,2048]{1,0:T(8,128)(2,1)}), bf16[256,2048]{1,0:T(8,128)(2,1)}) %all-reduce.6.cloned.1.call-update) | async-done | bytes 1048592 | tf_op jit(solution)/shard_map/psum | solution.py:16
  555.7 1.5 fusion.5
  557.2 1.9 fusion.18
  559.1 4.5 fusion.45
  563.6 0.0 copy-start.7
  563.6 8.9 %convolution_convert_fusion.1 = bf16[256,2048]{1,0:T(8,128)(2,1)} fusion(bf16[1408,2048]{1,0:T(8,128)(2,1)} %all-gather.11.cloned.1.call-done, bf16[2048,1408]{1,0:T(8,128)(2,1)} %all-gather.9.cloned.1.call-done, f32[256,1408]{1,0:T(8,128)S(1)} %fusion.45, bf16[256,2048]{1,0:T(8,128)(2,1)S(1)} %get-tuple-element.6, f32[2048]{0:T(1024)S(1)} %convert_element_type.99, ...), kind=kOutput, calls=%fused_computation.20 | convolution fusion | flops 2957574144 | bytes 15082496 | tf_op jit(solution)/shard_map/dot_general | solution.py:89
  572.5 0.0 all-reduce.8.cloned.1.call-update
  572.5 0.0 copy-done.7
  572.5 36.9 %all-reduce.8.cloned.1.call-done = bf16[256,2048]{1,0:T(8,128)(2,1)} async-done(((bf16[256,2048]{1,0:T(8,128)(2,1)}), bf16[256,2048]{1,0:T(8,128)(2,1)}) %all-reduce.8.cloned.1.call-update) | async-done | bytes 1048592 | tf_op jit(solution)/shard_map/psum | solution.py:16
  609.4 1.5 fusion.7
  610.9 2.8 fusion.21
  (22 shorter events, 0.1 us)
Async XLA Ops:
  6.5 2.3 copy-start.2
  6.5 2.3 copy-start
  6.5 111.8 %all-gather.7.cloned.1.call-start = ((), (), s32[]{:S(2)}) async-start(), calls=%async_computation | async-start | bytes 7208960 | tf_op jit(solution)/shard_map/all_gather | solution.py:69
  7.3 217.6 %all-gather.11.cloned.1.call-start = ((), (), s32[]{:S(2)}) async-start(), calls=%async_computation.2 | async-start | bytes 7208960 | tf_op jit(solution)/shard_map/all_gather | solution.py:72
  8.0 323.4 %all-gather.9.cloned.1.call-start = ((), (), s32[]{:S(2)}) async-start(), calls=%async_computation.1 | async-start | bytes 7208960 | tf_op jit(solution)/shard_map/all_gather | solution.py:70
  8.7 366.4 %all-reduce.4.cloned.1.call-start = ((), (), s32[]{:S(2)}) async-start(), calls=%async_computation.3 | async-start | bytes 2097152 | tf_op jit(solution)/shard_map/psum | solution.py:16
  340.4 2.2 copy-start.3
  340.4 2.2 copy-start.4
  340.4 2.2 copy-start.8
  340.4 2.3 copy-start.9
  340.4 82.3 %all-gather.15.cloned.1.call-start = ((), (), s32[]{:S(2)}) async-start(), calls=%async_computation.5 | async-start | bytes 2621440 | tf_op jit(solution)/shard_map/all_gather | solution.py:79
  341.0 127.6 %all-gather.13.cloned.1.call-start = ((), (), s32[]{:S(2)}) async-start(), calls=%async_computation.4 | async-start | bytes 2621440 | tf_op jit(solution)/shard_map/all_gather | solution.py:78
  341.6 173.1 %all-gather.17.cloned.1.call-start = ((), (), s32[]{:S(2)}) async-start(), calls=%async_computation.6 | async-start | bytes 2621440 | tf_op jit(solution)/shard_map/all_gather | solution.py:84
  342.3 213.3 %all-reduce.6.cloned.1.call-start = ((), (), s32[]{:S(2)}) async-start(), calls=%async_computation.7 | async-start | bytes 2097152 | tf_op jit(solution)/shard_map/psum | solution.py:16
  426.3 1.7 copy-start.1
  514.7 6.0 copy-start.5
  514.7 6.0 copy-start.6
  520.4 89.0 %all-reduce.8.cloned.1.call-start = ((), (), s32[]{:S(2)}) async-start(), calls=%async_computation.8 | async-start | bytes 2097152 | tf_op jit(solution)/shard_map/psum | solution.py:16
  563.6 9.0 %copy-start.7 = (bf16[2048]{0:T(1024)(128)(2,1)S(1)}, bf16[2048]{0:T(1024)(128)(2,1)}, u32[]{:S(2)}) copy-start(bf16[2048]{0:T(1024)(128)(2,1)} %param.31) | copy-start | bytes 12292
Sparse Core Ops, SparseCore 0:
  8.9 109.3 all-gather.6
  119.9 104.9 all-gather.10
  226.5 104.9 all-gather.8
  340.5 34.5 all-reduce.3
  376.5 46.1 all-gather.14
  424.1 44.4 all-gather.12
  470.2 44.4 all-gather.16
  520.5 35.0 all-reduce.5
  572.6 36.7 all-reduce.7
where the time goes:
time: 621 us; the launch traced here: 620 us
  waiting for transfers between devices  556 us (90%)
  matrix products  36.2 us (6%)
  between operations  13.5 us (2%)
  other arithmetic  12.6 us (2%)
    all_gather x1, waiting for transfers between devices, shards(): lax.all_gather(gate_weight, 'fs', axis=0, tiled=True)  109 us
    all_gather x1, waiting for transfers between devices, shards(): lax.all_gather(up_weight, 'fs', axis=0, tiled=True)  107 us
    psum x3, waiting for transfers between devices, reduce_partial(): return lax.psum(terms.astype(jnp.bfloat16), 'tp').astype(jnp.float32)  104 us
    all_gather x1, waiting for transfers between devices, shards(): down_full = lax.all_gather(down_weight, 'fs', axis=1, tiled=True)  102 us
    all_gather x1, waiting for transfers between devices, shards(): out_full = lax.all_gather(mix_out_weight, 'fs', axis=1, tiled=True)  46.1 us
    all_gather x1, waiting for transfers between devices, shards(): lax.all_gather(mix_v_weight, 'fs', axis=0, tiled=True)  44.1 us
    all_gather x1, waiting for transfers between devices, shards(): lax.all_gather(mix_u_weight, 'fs', axis=0, tiled=True)  40.1 us
    dot_general x2, matrix products, shards(): terms = jnp.dot(hidden, down_full, preferred_element_type=jnp.float32)  17.8 us
  transfers between devices with their start and end apart: 9, of which 9 were waited for; matrix products, arithmetic and copies ran while one was open for 2% of the time, Pallas kernels for 0%

commit v1 on v0

--- a/solution.py
+++ b/solution.py
@@ -69,7 +69,13 @@
         lax.all_gather(gate_weight, "fs", axis=0, tiled=True),
         lax.all_gather(up_weight, "fs", axis=0, tiled=True),
     )
-    down_full = lax.all_gather(down_weight, "fs", axis=1, tiled=True)
+    peers = lax.axis_size("fs")
+    held, pieces = (down_weight, [down_weight])
+    for _ in range(peers - 1):
+        held = lax.ppermute(held, "fs", [(i, (i + 1) % peers) for i in range(peers)])
+        pieces.insert(0, held)
+    line = jnp.concatenate(pieces, axis=1)
+    down_full = jnp.roll(line, (lax.axis_index("fs") + 1) * down_weight.shape[1], axis=1)
     hidden = gated_hidden(normed, gate_full, up_full)
     terms = jnp.dot(hidden, down_full, preferred_element_type=jnp.float32)
     first = add_branch(tokens, terms, ffn_post_gain, 0.5)

time: 621 us -> 585 us (0.942)
  waiting for transfers between devices: 556 us -> 459 us
  starting transfers between devices: 0.71 us -> 43 us
  local copies, waits for them, and re-layouts: 1.03 us -> 17.2 us
    ppermute x0 -> x3, waiting for transfers between devices: none -> 170 us  [shards(): lax.ppermute(held, 'fs', [(i, (i + 1) % peers) for i in range(peers)])]
    all_gather x1, waiting for transfers between devices: 109 us -> 0.01 us  [shards(): lax.all_gather(gate_weight, 'fs', axis=0, tiled=True)]
    all_gather x1 -> x0, waiting for transfers between devices: 102 us -> none  [shards(): down_full = lax.all_gather(down_weight, 'fs', axis=1, tiled=True)]
    all_gather x1, waiting for transfers between devices: 107 us -> 51.8 us  [shards(): lax.all_gather(up_weight, 'fs', axis=0, tiled=True)]
    ppermute x0 -> x3, starting transfers between devices: none -> 42.3 us  [shards(): lax.ppermute(held, 'fs', [(i, (i + 1) % peers) for i in range(peers)])]
    unnamed x20 -> x37, local copies, waits for them, and re-layouts: 0.04 us -> 15 us
  transfers between devices with their start and end apart: 9 -> 11, of which waited for: 9 -> 10; matrix products, arithmetic and copies ran while one was open for 2% -> 5% of each run, Pallas kernels for 0% -> 0%
where the time goes in v1:
time: 585 us; the launch traced here: 584 us
  waiting for transfers between devices  459 us (78%)
  starting transfers between devices  43 us (7%)
  matrix products  36.1 us (6%)
  local copies, waits for them, and re-layouts  17.2 us (3%)
  other arithmetic  14.9 us (3%)
  between operations  13.8 us (2%)
    ppermute x3, waiting for transfers between devices, shards(): lax.ppermute(held, 'fs', [(i, (i + 1) % peers) for i in range(peers)])  170 us
    psum x3, waiting for transfers between devices, reduce_partial(): return lax.psum(terms.astype(jnp.bfloat16), 'tp').astype(jnp.float32)  104 us
    all_gather x1, waiting for transfers between devices, shards(): lax.all_gather(up_weight, 'fs', axis=0, tiled=True)  51.8 us
    all_gather x1, waiting for transfers between devices, shards(): out_full = lax.all_gather(mix_out_weight, 'fs', axis=1, tiled=True)  45.9 us
    all_gather x1, waiting for transfers between devices, shards(): lax.all_gather(mix_v_weight, 'fs', axis=0, tiled=True)  44.1 us
    ppermute x3, starting transfers between devices, shards(): lax.ppermute(held, 'fs', [(i, (i + 1) % peers) for i in range(peers)])  42.3 us
    all_gather x1, waiting for transfers between devices, shards(): lax.all_gather(mix_u_weight, 'fs', axis=0, tiled=True)  40.1 us
    dot_general x2, matrix products, shards(): terms = jnp.dot(hidden, down_full, preferred_element_type=jnp.float32)  17.8 us
  transfers between devices with their start and end apart: 11, of which 10 were waited for; matrix products, arithmetic and copies ran while one was open for 5% of the time, Pallas kernels for 0%

profile of v1, /device:TPU:0, one launch (start us, length us, event | category | flops | bytes accessed | tf_op | source)
XLA Modules:
  0.0 584.5 jit_solution(8035746232281083722)
XLA Ops:
  6.5 0.7 all-gather.6.cloned.1.call-update
  7.3 0.0 all-gather.8.cloned.1.call-start
  7.3 0.7 all-gather.8.cloned.1.call-update
  8.0 0.0 all-reduce.4.cloned.1.call-start
  8.1 3.1 collective-permute-start
  11.2 54.4 %collective-permute-done = bf16[1408,512]{1,0:T(8,128)(2,1)S(1)} collective-permute-done((bf16[1408,512]{1,0:T(8,128)(2,1)S(1)}, bf16[1408,512]{1,0:T(8,128)(2,1)S(1)}, u32[]{:S(2)}, u32[]{:S(2)}) %collective-permute-start) | collective-permute-done | bytes 1441824 | tf_op jit(solution)/shard_map/ppermute | solution.py:75
  65.5 23.7 %collective-permute-start.1 = (bf16[1408,512]{1,0:T(8,128)(2,1)S(1)}, bf16[1408,512]{1,0:T(8,128)(2,1)}, u32[]{:S(2)}, u32[]{:S(2)}) collective-permute-start(bf16[1408,512]{1,0:T(8,128)(2,1)S(1)} %collective-permute-done), channel_id=1, source_target_pairs={{0,4},{4,8},{8,12},{12,0},{1,5},{5,9},{9,13},{13,1},{2,6},{6,10},{... | collective-permute-start | bytes 4325384 | tf_op jit(solution)/shard_map/ppermute | solution.py:75
  89.3 62.4 %collective-permute-done.1 = bf16[1408,512]{1,0:T(8,128)(2,1)} collective-permute-done((bf16[1408,512]{1,0:T(8,128)(2,1)S(1)}, bf16[1408,512]{1,0:T(8,128)(2,1)}, u32[]{:S(2)}, u32[]{:S(2)}) %collective-permute-start.1) | collective-permute-done | bytes 1441824 | tf_op jit(solution)/shard_map/ppermute | solution.py:75
  151.7 15.5 %collective-permute-start.2 = (bf16[1408,512]{1,0:T(8,128)(2,1)}, bf16[1408,512]{1,0:T(8,128)(2,1)}, u32[]{:S(2)}, u32[]{:S(2)}) collective-permute-start(bf16[1408,512]{1,0:T(8,128)(2,1)} %collective-permute-done.1), channel_id=1, source_target_pairs={{0,4},{4,8},{8,12},{12,0},{1,5},{5,9},{9,13},{13,1},{2,6},{6,10},{... | collective-permute-start | bytes 4325384 | tf_op jit(solution)/shard_map/ppermute | solution.py:75
  167.2 1.5 fusion.20
  168.7 53.5 %collective-permute-done.2 = bf16[1408,512]{1,0:T(8,128)(2,1)} collective-permute-done((bf16[1408,512]{1,0:T(8,128)(2,1)}, bf16[1408,512]{1,0:T(8,128)(2,1)}, u32[]{:S(2)}, u32[]{:S(2)}) %collective-permute-start.2) | collective-permute-done | bytes 1441824 | tf_op jit(solution)/shard_map/ppermute | solution.py:75
  222.2 2.7 constant_dynamic-update-slice_fusion.7
  224.9 2.7 constant_dynamic-update-slice_fusion.6
  227.5 1.2 constant_dynamic-update-slice_fusion.5
  228.8 1.3 constant_dynamic-update-slice_fusion.4
  230.0 2.7 constant_dynamic-update-slice_fusion.3
  232.7 2.6 constant_dynamic-update-slice_fusion.2
  235.4 1.3 constant_dynamic-update-slice_fusion.1
  236.7 1.3 constant_dynamic-update-slice_fusion
  238.0 0.5 copy-done.1
  238.4 4.5 fusion.69
  242.9 51.8 %all-gather.8.cloned.1.call-done = bf16[2048,1408]{1,0:T(8,128)(2,1)} async-done(((bf16[512,1408]{1,0:T(8,128)(2,1)}), bf16[2048,1408]{1,0:T(8,128)(2,1)}) %all-gather.8.cloned.1.call-update) | async-done | bytes 5767184 | tf_op jit(solution)/shard_map/all_gather | solution.py:70
  294.7 8.8 %fusion.6 = bf16[256,2048]{1,0:T(8,128)(2,1)} fusion(bf16[1408,4096]{1,0:T(8,128)(2,1)} %constant_dynamic-update-slice_fusion, s32[]{:T(128)S(6)} %select_n.20, bf16[2048,1408]{1,0:T(8,128)(2,1)} %all-gather.8.cloned.1.call-done, f32[256,1408]{1,0:T(8,128)S(1)} %fusion.69, bf16[256,2048]{1,0:T(8,128)(2,1)S(1)} %copy-done.1, ...), kind=kOutput, calls=%fused_computation.24 | convolution fusion | flops 2957574144 | bytes 15082500 | tf_op jit(solution)/shard_map/dot_general | solution.py:80
  303.6 0.0 all-reduce.4.cloned.1.call-update
  303.6 0.0 all-gather.12.cloned.1.call-start
  303.6 0.5 all-gather.12.cloned.1.call-update
  304.2 0.0 all-gather.10.cloned.1.call-start
  304.2 0.5 all-gather.10.cloned.1.call-update
  304.8 0.0 all-gather.14.cloned.1.call-start
  304.8 0.5 all-gather.14.cloned.1.call-update
  305.3 0.2 all-reduce.6.cloned.1.call-start
  305.7 0.6 bitcast_convert_fusion
  306.2 0.6 convert_bitcast_fusion
  306.8 32.3 %all-reduce.4.cloned.1.call-done = bf16[256,2048]{1,0:T(8,128)(2,1)} async-done(((bf16[256,2048]{1,0:T(8,128)(2,1)}), bf16[256,2048]{1,0:T(8,128)(2,1)}) %all-reduce.4.cloned.1.call-update) | async-done | bytes 1048592 | tf_op jit(solution)/shard_map/psum | solution.py:16
  339.1 1.5 fusion.12
  340.6 2.0 fusion.24
  342.6 44.1 %all-gather.12.cloned.1.call-done = bf16[2048,512]{1,0:T(8,128)(2,1)} async-done(((bf16[512,512]{1,0:T(8,128)(2,1)}), bf16[2048,512]{1,0:T(8,128)(2,1)}) %all-gather.12.cloned.1.call-update) | async-done | bytes 2097168 | tf_op jit(solution)/shard_map/all_gather | solution.py:85
  386.7 3.4 fusion.38
  390.1 0.2 reshape.99
  390.3 0.0 copy-start.2
  390.3 0.2 reshape.98
  390.5 0.3 reduce_sum.75
  390.9 0.6 multiply_reduce_fusion
  391.5 0.1 copy.36
  391.6 0.2 copy.25
  391.9 0.1 copy.37
  391.9 0.0 copy-done.4
  391.9 0.3 fusion.32
  392.2 0.2 copy.28
  392.5 40.1 %all-gather.10.cloned.1.call-done = bf16[2048,512]{1,0:T(8,128)(2,1)} async-done(((bf16[512,512]{1,0:T(8,128)(2,1)}), bf16[2048,512]{1,0:T(8,128)(2,1)}) %all-gather.10.cloned.1.call-update) | async-done | bytes 2097168 | tf_op jit(solution)/shard_map/all_gather | solution.py:84
  432.6 45.9 %all-gather.14.cloned.1.call-done = bf16[512,2048]{1,0:T(8,128)(2,1)} async-done(((bf16[512,512]{1,0:T(8,128)(2,1)}), bf16[512,2048]{1,0:T(8,128)(2,1)}) %all-gather.14.cloned.1.call-update) | async-done | bytes 2097168 | tf_op jit(solution)/shard_map/all_gather | solution.py:90
  478.5 5.7 convolution_convert_fusion
  484.2 0.0 all-reduce.6.cloned.1.call-update
  484.3 0.3 all-reduce.8.cloned.1.call-start
  484.6 35.0 %all-reduce.6.cloned.1.call-done = bf16[256,2048]{1,0:T(8,128)(2,1)} async-done(((bf16[256,2048]{1,0:T(8,128)(2,1)}), bf16[256,2048]{1,0:T(8,128)(2,1)}) %all-reduce.6.cloned.1.call-update) | async-done | bytes 1048592 | tf_op jit(solution)/shard_map/psum | solution.py:16
  519.5 1.5 fusion.15
  521.1 1.9 fusion.28
  522.9 4.5 fusion.55
  527.4 0.0 copy-start.12
  527.5 9.0 %fusion.9 = bf16[256,2048]{1,0:T(8,128)(2,1)} fusion(bf16[1408,4096]{1,0:T(8,128)(2,1)} %constant_dynamic-update-slice_fusion, s32[]{:T(128)S(6)} %select_n.20, bf16[2048,1408]{1,0:T(8,128)(2,1)} %all-gather.8.cloned.1.call-done, f32[256,1408]{1,0:T(8,128)S(1)} %fusion.55, bf16[256,2048]{1,0:T(8,128)(2,1)S(1)} %get-tuple-element.6, ...), kind=kOutput, calls=%fused_computation.25 | convolution fusion | flops 2957574144 | bytes 15082500 | tf_op jit(solution)/shard_map/dot_general | solution.py:95
  536.4 0.0 all-reduce.8.cloned.1.call-update
  536.5 36.9 %all-reduce.8.cloned.1.call-done = bf16[256,2048]{1,0:T(8,128)(2,1)} async-done(((bf16[256,2048]{1,0:T(8,128)(2,1)}), bf16[256,2048]{1,0:T(8,128)(2,1)}) %all-reduce.8.cloned.1.call-update) | async-done | bytes 1048592 | tf_op jit(solution)/shard_map/psum | solution.py:16
  573.4 1.5 fusion.17
  574.9 2.8 fusion.31
  (43 shorter events, 0.2 us)
Async XLA Ops:
  6.5 1.5 copy-start
  6.5 160.6 %copy-start.7 = (bf16[2048]{0:T(1024)(128)(2,1)S(1)}, bf16[2048]{0:T(1024)(128)(2,1)}, u32[]{:S(2)}) copy-start(bf16[2048]{0:T(1024)(128)(2,1)} %param.17) | copy-start | bytes 12292
  6.5 231.4 %all-gather.6.cloned.1.call-start = ((), (), s32[]{:S(2)}) async-start(), calls=%async_computation | async-start | bytes 7208960 | tf_op jit(solution)/shard_map/all_gather | solution.py:69
  7.3 287.5 %all-gather.8.cloned.1.call-start = ((), (), s32[]{:S(2)}) async-start(), calls=%async_computation.1 | async-start | bytes 7208960 | tf_op jit(solution)/shard_map/all_gather | solution.py:70
  8.0 331.1 %all-reduce.4.cloned.1.call-start = ((), (), s32[]{:S(2)}) async-start(), calls=%async_computation.2 | async-start | bytes 2097152 | tf_op jit(solution)/shard_map/psum | solution.py:16
  8.1 57.5 %collective-permute-start = (bf16[1408,512]{1,0:T(8,128)(2,1)S(1)}, bf16[1408,512]{1,0:T(8,128)(2,1)S(1)}, u32[]{:S(2)}, u32[]{:S(2)}) collective-permute-start(bf16[1408,512]{1,0:T(8,128)(2,1)S(1)} %copy-done), channel_id=1, source_target_pairs={{0,4},{4,8},{8,12},{12,0},{1,5},{5,9},{9,13},{13,1},{2,6},{6,10},{... | collective-permute-start | bytes 4325384 | tf_op jit(solution)/shard_map/ppermute | solution.py:75
  65.5 86.2 %collective-permute-start.1 = (bf16[1408,512]{1,0:T(8,128)(2,1)S(1)}, bf16[1408,512]{1,0:T(8,128)(2,1)}, u32[]{:S(2)}, u32[]{:S(2)}) collective-permute-start(bf16[1408,512]{1,0:T(8,128)(2,1)S(1)} %collective-permute-done), channel_id=1, source_target_pairs={{0,4},{4,8},{8,12},{12,0},{1,5},{5,9},{9,13},{13,1},{2,6},{6,10},{... | collective-permute-start | bytes 4325384 | tf_op jit(solution)/shard_map/ppermute | solution.py:75
  151.7 70.5 %collective-permute-start.2 = (bf16[1408,512]{1,0:T(8,128)(2,1)}, bf16[1408,512]{1,0:T(8,128)(2,1)}, u32[]{:S(2)}, u32[]{:S(2)}) collective-permute-start(bf16[1408,512]{1,0:T(8,128)(2,1)} %collective-permute-done.1), channel_id=1, source_target_pairs={{0,4},{4,8},{8,12},{12,0},{1,5},{5,9},{9,13},{13,1},{2,6},{6,10},{... | collective-permute-start | bytes 4325384 | tf_op jit(solution)/shard_map/ppermute | solution.py:75
  236.7 1.8 copy-start.1
  303.6 2.0 copy-start.8
  303.6 2.0 copy-start.9
  303.6 2.1 copy-start.13
  303.6 2.7 copy-start.14
  303.6 83.1 %all-gather.12.cloned.1.call-start = ((), (), s32[]{:S(2)}) async-start(), calls=%async_computation.4 | async-start | bytes 2621440 | tf_op jit(solution)/shard_map/all_gather | solution.py:85
  304.2 128.4 %all-gather.10.cloned.1.call-start = ((), (), s32[]{:S(2)}) async-start(), calls=%async_computation.3 | async-start | bytes 2621440 | tf_op jit(solution)/shard_map/all_gather | solution.py:84
  304.8 173.8 %all-gather.14.cloned.1.call-start = ((), (), s32[]{:S(2)}) async-start(), calls=%async_computation.5 | async-start | bytes 2621440 | tf_op jit(solution)/shard_map/all_gather | solution.py:90
  305.3 214.2 %all-reduce.6.cloned.1.call-start = ((), (), s32[]{:S(2)}) async-start(), calls=%async_computation.6 | async-start | bytes 2097152 | tf_op jit(solution)/shard_map/psum | solution.py:16
  305.6 81.1 %copy-start.5 = (f32[2048]{0:T(1024)}, f32[2048]{0:T(1024)S(1)}, u32[]{:S(2)}) copy-start(f32[2048]{0:T(1024)S(1)} %convert_element_type.90) | copy-start | bytes 24580
  390.3 1.7 copy-start.2
  390.3 1.7 copy-start.3
  390.3 1.6 copy-start.4
  391.5 87.0 %copy-start.6 = (f32[2048]{0:T(1024)S(1)}, f32[2048]{0:T(1024)}, u32[]{:S(2)}) copy-start(f32[2048]{0:T(1024)} %copy-done.5) | copy-start | bytes 24580
  478.5 6.0 %copy-start.10 = (bf16[2048]{0:T(1024)(128)(2,1)S(1)}, bf16[2048]{0:T(1024)(128)(2,1)}, u32[]{:S(2)}) copy-start(bf16[2048]{0:T(1024)(128)(2,1)} %param.29) | copy-start | bytes 12292
  478.5 6.0 %copy-start.11 = (bf16[2048]{0:T(1024)(128)(2,1)S(1)}, bf16[2048]{0:T(1024)(128)(2,1)}, u32[]{:S(2)}) copy-start(bf16[2048]{0:T(1024)(128)(2,1)} %param.30) | copy-start | bytes 12292
  484.3 89.1 %all-reduce.8.cloned.1.call-start = ((), (), s32[]{:S(2)}) async-start(), calls=%async_computation.7 | async-start | bytes 2097152 | tf_op jit(solution)/shard_map/psum | solution.py:16
  527.4 9.0 %copy-start.12 = (bf16[2048]{0:T(1024)(128)(2,1)S(1)}, bf16[2048]{0:T(1024)(128)(2,1)}, u32[]{:S(2)}) copy-start(bf16[2048]{0:T(1024)(128)(2,1)} %param.31) | copy-start | bytes 12292
Sparse Core Ops, SparseCore 0:
  8.9 159.9 all-gather.5
  170.5 124.1 all-gather.7
  303.7 35.3 all-reduce.3
  340.5 46.1 all-gather.11
  388.1 44.4 all-gather.9
  434.0 44.4 all-gather.13
  484.4 35.1 all-reduce.5
  536.6 36.7 all-reduce.7
